TPU v7x, 512 devices: a whole 4x4x16 slice. The times are simulated.
512 devices in a mesh: ep: 128 (over z, x, core), tp: 4 (over y).
Axes of the slice: x: 4, y: 4, z: 16, core: 2. Of those that a mesh axis runs over, the one named last changes fastest.
Arguments:
- tokens: bfloat16 [1024, 2048], P('ep'), may hold values from -6 to 6
- norm_gain: float32 [2048], replicated, may hold values from 0.1 to 1.9
- query_weight: bfloat16 [2048, 1024], P('ep', 'tp'), may hold values from -0.125 to 0.125
- key_weight: bfloat16 [2048, 512], P('ep', 'tp'), may hold values from -0.125 to 0.125
- value_weight: bfloat16 [2048, 512], P('ep', 'tp'), may hold values from -0.125 to 0.125
- query_gain: float32 [64], replicated, may hold values from 0.9 to 1.9
- key_gain: float32 [64], replicated, may hold values from 0.9 to 1.9
- lambdas: float32 [8], P('tp'), may hold values from 0.3 to 0.8
- key_cache: bfloat16 [1024, 4, 320, 128], P('ep', 'tp'), may hold values from -5 to 5
- value_cache: bfloat16 [1024, 4, 320, 128], P('ep', 'tp'), may hold values from -6 to 6
- lengths: int32 [1024], P('ep'), may hold values from 1 to 320
- head_gain: float32 [128], replicated, may hold values from 0.1 to 1.9
- out_weight: bfloat16 [1024, 2048], P('tp', 'ep'), may hold values from -0.1875 to 0.1875
- ffn_gain: float32 [2048], replicated, may hold values from 0.1 to 1.9
- dense_gate_weight: bfloat16 [2048, 1024], P('ep', 'tp'), may hold values from -0.125 to 0.125
- dense_up_weight: bfloat16 [2048, 1024], P('ep', 'tp'), may hold values from -0.125 to 0.125
- dense_down_weight: bfloat16 [1024, 2048], P('tp', 'ep'), may hold values from -0.1875 to 0.1875
- branch_gate: float32 [2048], replicated, may hold values from -0.125 to 0.125
- expert_ids: int32 [1024, 2], P('ep'), may hold values from 0 to 15, all different within a row; in each aligned block of 8 rows (0 to 7, 8 to 15, ...) at most 2 rows name the same one
- expert_probs: float32 [1024, 2], P('ep'), may hold values from 0.1 to 0.9
- expert_gate: bfloat16 [128, 2048, 704], P('ep', None, 'tp'), may hold values from -0.125 to 0.125
- expert_up: bfloat16 [128, 2048, 704], P('ep', None, 'tp'), may hold values from -0.125 to 0.125
- expert_down: bfloat16 [128, 704, 2048], P('ep', 'tp'), may hold values from -0.078125 to 0.078125
Outputs:
- mixed: bfloat16 [1024, 2048], P('ep', 'tp')
Inputs may be any that keep to these rules, and one draw needn't show every extreme that they name: `expert_ids`: each row names 2 different experts. Within each aligned block of 8 rows (the sequences of one index of ep) no expert is named more than 2 times, and in every draw some block names some expert exactly 2 times.
All inputs are finite; a program needn't handle non-finite values.
Results may differ from a plain program's by a relative error of at most 0.014.
Values may be sent and summed in bfloat16 or wider, within the bound.
No kernel may reach another device: no remote copies, remote signals or barrier semaphores. Data moves between devices by JAX's collectives and lax.ppermute only.
A program may use at most 64 MiB of HBM per device.

v0:
```python
import jax
import jax.numpy as jnp
from jax import lax
from jax.sharding import Mesh, PartitionSpec as P

SUB = 64
VD = 128
EXPERTS = 16
TOP = 2
CAP = 2
REP = 8
N_Z = 16
N_XC = 8
N_EP = 128
N_TP = 4
SEQ = 8
EP = ("b", "zp", "x", "c")
Z = ("b", "zp")
XC = ("x", "c")
epsilon = 1e-06


def rms_scale(values, scaling):
    return values * lax.rsqrt(jnp.mean(values * values, axis=-1, keepdims=True) + epsilon) * scaling


def exchange(values, axes):
    return lax.all_to_all(values, axes, split_axis=0, concat_axis=0, tiled=True)


def gather_small(values, axes, count):
    return exchange(jnp.broadcast_to(values[None], (count,) + values.shape), axes)


def to_mixed(rows):
    count = rows.shape[0]
    return rows.reshape(count, N_Z, N_XC, -1).transpose(0, 2, 1, 3).reshape(count, -1)


def from_mixed(rows):
    count = rows.shape[0]
    return rows.reshape(count, N_XC, N_Z, -1).transpose(0, 2, 1, 3).reshape(count, -1)


def attend(packed, key_cache, value_cache, lengths, query_gain, key_gain, lambdas, head_gain):
    seq_here = packed.shape[0]
    kv_here = key_cache.shape[1]
    cache_len = key_cache.shape[2]
    heads_here = lambdas.shape[0]
    per_group = heads_here // kv_here
    query_end = heads_here * 2 * SUB
    key_end = query_end + kv_here * 2 * SUB
    mixed = lax.optimization_barrier(packed.astype(jnp.bfloat16))
    query_parts = rms_scale(
        mixed[:, :query_end].astype(jnp.float32).reshape(seq_here, kv_here, per_group, 2, SUB),
        query_gain,
    ).astype(jnp.bfloat16)
    key_parts = rms_scale(
        mixed[:, query_end:key_end].astype(jnp.float32).reshape(seq_here, kv_here, 2, SUB), key_gain
    ).astype(jnp.bfloat16)
    new_values = mixed[:, key_end:].reshape(seq_here, kv_here, VD)
    cached = rms_scale(
        key_cache.astype(jnp.float32).reshape(seq_here, kv_here, cache_len, 2, SUB), key_gain
    ).astype(jnp.bfloat16)
    score_scale = SUB ** (-0.5)
    scores = (
        jnp.einsum("sgqcd,sgjcd->sgqcj", query_parts, cached, preferred_element_type=jnp.float32)
        * score_scale
    )
    own_score = (
        jnp.einsum("sgqcd,sgcd->sgqc", query_parts, key_parts, preferred_element_type=jnp.float32)
        * score_scale
    )
    live_mask = lax.broadcasted_iota(jnp.int32, (seq_here, cache_len), 1) < lengths[:, None]
    exponent = jnp.where(live_mask[:, None, None, None, :], jnp.exp(scores), 0.0)
    own_exponent = jnp.exp(own_score)
    denominator = jnp.sum(exponent, axis=4) + own_exponent
    shares = exponent / denominator[..., None]
    own_shares = own_exponent / denominator
    lam_heads = lambdas.reshape(1, kv_here, per_group)
    mixing = (shares[:, :, :, 0] - lam_heads[..., None] * shares[:, :, :, 1]).astype(jnp.bfloat16)
    own_mixing = lax.optimization_barrier(
        (own_shares[:, :, :, 0] - lam_heads * own_shares[:, :, :, 1]).astype(jnp.bfloat16)
    )
    head_out = jnp.einsum(
        "sgqj,sgje->sgqe", mixing, value_cache, preferred_element_type=jnp.float32
    )
    head_out = (
        head_out
        + own_mixing.astype(jnp.float32)[..., None] * new_values.astype(jnp.float32)[:, :, None, :]
    )
    return rms_scale(head_out, head_gain).astype(jnp.bfloat16).reshape(seq_here, heads_here * VD)


def route_tables(expert_ids, expert_probs):
    seq_here = expert_ids.shape[0]
    paired = expert_ids.reshape(-1)
    total_pairs = paired.shape[0]
    onehot = (paired[:, None] == lax.broadcasted_iota(jnp.int32, (total_pairs, EXPERTS), 1)).astype(
        jnp.float32
    )
    earlier = (
        lax.broadcasted_iota(jnp.int32, (total_pairs, total_pairs), 1)
        < lax.broadcasted_iota(jnp.int32, (total_pairs, total_pairs), 0)
    ).astype(jnp.float32)
    before = jnp.dot(earlier, onehot, precision=lax.Precision.HIGHEST)
    slot_ranks = jnp.sum(before * onehot, axis=1).astype(jnp.int32)
    slot_codes = (paired * CAP + slot_ranks).reshape(seq_here, TOP)
    slots_iota = lax.broadcasted_iota(jnp.int32, (seq_here, TOP, EXPERTS * CAP), 2)
    picked = (slot_codes[:, :, None] == slots_iota).astype(jnp.float32)
    select = jnp.sum(picked, axis=1)
    combine_weights = jnp.sum(picked * expert_probs[:, :, None], axis=1)
    return (select, combine_weights)


def own_columns(values, tp_start, share_width):
    return lax.dynamic_slice_in_dim(values, tp_start, share_width, 1)


def shards(
    tokens,
    norm_gain,
    query_weight,
    key_weight,
    value_weight,
    query_gain,
    key_gain,
    lambdas,
    key_cache,
    value_cache,
    lengths,
    head_gain,
    out_weight,
    ffn_gain,
    dense_gate_weight,
    dense_up_weight,
    dense_down_weight,
    branch_gate,
    expert_ids,
    expert_probs,
    expert_gate,
    expert_up,
    expert_down,
):
    residual = tokens.astype(jnp.float32)
    normed = rms_scale(residual, norm_gain).astype(jnp.bfloat16)
    width = residual.shape[1]
    share_width = width // N_TP
    tp_start = lax.axis_index("tp") * share_width
    spread = exchange(
        to_mixed(normed).reshape(SEQ, N_XC, width // N_XC).transpose(1, 0, 2), XC
    ).reshape(N_XC * SEQ, width // N_XC)
    shard = jnp.concatenate(
        (
            query_weight,
            key_weight,
            value_weight,
            out_weight.T,
            dense_gate_weight,
            dense_up_weight,
            dense_down_weight.T,
        ),
        axis=1,
    )
    held = lax.all_gather(shard, Z, axis=0, tiled=True)
    out_held = lax.all_gather(held[:, 512:768], XC, axis=0, tiled=True)
    dense_held = lax.all_gather(held[:, 768:], XC, axis=0, tiled=True)
    partial_rows = jnp.dot(spread, held[:, :512], preferred_element_type=jnp.float32)
    packed = jnp.sum(exchange(partial_rows.reshape(N_XC, SEQ, 512), XC), axis=0)
    head_out = attend(
        packed, key_cache, value_cache, lengths, query_gain, key_gain, lambdas, head_gain
    )
    attended_part = from_mixed(
        lax.dot_general(
            head_out, out_held, (((1,), (1,)), ((), ())), preferred_element_type=jnp.float32
        ).astype(jnp.bfloat16)
    )
    attended = jnp.sum(gather_small(attended_part, "tp", N_TP).astype(jnp.float32), axis=0)
    middle = lax.optimization_barrier((residual + attended).astype(jnp.bfloat16))
    middle_f32 = middle.astype(jnp.float32)
    ffn_input = lax.optimization_barrier(rms_scale(middle_f32, ffn_gain).astype(jnp.bfloat16))
    select, combine_weights = route_tables(expert_ids, expert_probs)
    ffn_share = own_columns(ffn_input, tp_start, share_width)
    chosen = jnp.dot(
        select.astype(jnp.bfloat16).T, ffn_share, preferred_element_type=jnp.float32
    ).astype(jnp.bfloat16)
    outgoing = jnp.broadcast_to(
        chosen.reshape(1, EXPERTS, CAP, share_width), (REP, EXPERTS, CAP, share_width)
    ).reshape(N_EP, CAP, share_width)
    incoming = exchange(outgoing, EP).reshape(N_EP * CAP, share_width)
    dense_both = jnp.dot(
        to_mixed(ffn_input), dense_held[:, :512], preferred_element_type=jnp.float32
    )
    dense_hidden = (jax.nn.silu(dense_both[:, :256]) * dense_both[:, 256:]).astype(jnp.bfloat16)
    dense_part = from_mixed(
        lax.dot_general(
            dense_hidden,
            dense_held[:, 512:],
            (((1,), (1,)), ((), ())),
            preferred_element_type=jnp.float32,
        ).astype(jnp.bfloat16)
    )
    branch_weight = jax.nn.sigmoid(
        jnp.sum(ffn_input.astype(jnp.float32) * branch_gate, axis=1, keepdims=True)
    )
    rows = gather_small(incoming, "tp", N_TP)
    rows = rows.transpose(1, 0, 2).reshape(N_EP * CAP, width)
    gate_val = jnp.dot(rows, expert_gate[0], preferred_element_type=jnp.float32)
    up_val = jnp.dot(rows, expert_up[0], preferred_element_type=jnp.float32)
    hidden = (jax.nn.silu(gate_val) * up_val).astype(jnp.bfloat16)
    expert_part = jnp.dot(hidden, expert_down[0], preferred_element_type=jnp.float32).astype(
        jnp.bfloat16
    )
    both_parts = jnp.concatenate((expert_part, dense_part), axis=0)
    both_parts = both_parts.reshape(N_EP * CAP + SEQ, N_TP, share_width).transpose(1, 0, 2)
    summed = jnp.sum(exchange(both_parts, "tp").astype(jnp.float32), axis=0)
    block_out = summed[: N_EP * CAP].astype(jnp.bfloat16).reshape(N_EP, CAP, share_width)
    dense = summed[N_EP * CAP :]
    returned = exchange(block_out, EP)
    expert_out = jnp.sum(
        returned.reshape(REP, EXPERTS * CAP, share_width).astype(jnp.float32), axis=0
    )
    routed = jnp.dot(combine_weights, expert_out, precision=lax.Precision.HIGHEST)
    combined = own_columns(middle_f32, tp_start, share_width) + branch_weight * dense + routed
    return combined.astype(jnp.bfloat16)


def solution(mesh):
    fine = Mesh(mesh.devices.reshape(8, 2, 4, 2, 4), ("b", "zp", "x", "c", "tp"))
    return jax.shard_map(
        shards,
        mesh=fine,
        in_specs=(
            P(EP, None),
            P(),
            P(EP, "tp"),
            P(EP, "tp"),
            P(EP, "tp"),
            P(),
            P(),
            P("tp"),
            P(EP, "tp", None, None),
            P(EP, "tp", None, None),
            P(EP),
            P(),
            P("tp", EP),
            P(),
            P(EP, "tp"),
            P(EP, "tp"),
            P("tp", EP),
            P(),
            P(EP, None),
            P(EP, None),
            P(EP, None, "tp"),
            P(EP, None, "tp"),
            P(EP, "tp", None),
        ),
        out_specs=P(EP, "tp"),
        check_vma=False,
    )
```

profile of v0, /device:TPU:33, one launch (start us, length us, event | category | flops | bytes accessed | tf_op | source)
XLA Modules:
  0.0 216.1 jit_solution(8337824748790621756)
XLA Ops:
  11.5 30.8 %all_gather.9 = bf16[256,1536]{1,0:T(8,128)(2,1)S(1)} all-gather(bf16[16,1536]{1,0:T(8,128)(2,1)S(1)} %constant_dynamic-update-slice_fusion), channel_id=1, replica_groups=mesh['b'=8,'zp'=2,'x'=4,'c'=2,'tp'=4] {'b','zp'}, dimensions={0}, use_global_device_ids=true | all-gather | bytes 835584 | tf_op jit(solution)/shard_map/all_gather | solution.py:165
  43.0 0.9 fusion.25
  45.8 11.8 %all-to-all-start = ((bf16[8,8,256]{2,1,0:T(8,128)(2,1)}), bf16[8,8,256]{2,1,0:T(8,128)(2,1)S(1)}, u32[]{:S(2)}, u32[]{:S(2)}) async-start(bf16[8,8,256]{2,1,0:T(8,128)(2,1)} %bitcast.3), calls=%async_computation | async-start | bytes 65536 | tf_op jit(solution)/shard_map/all_to_all | solution.py:28
  58.5 1.2 copy.94
  59.6 1.3 convert_multiply_fusion
  63.2 4.1 %all-to-all-start.1 = ((f32[8,8,512]{2,1,0:T(8,128)}), f32[8,8,512]{2,1,0:T(8,128)S(1)}, u32[]{:S(2)}, u32[]{:S(2)}) async-start(f32[8,8,512]{2,1,0:T(8,128)} %fusion.18), calls=%async_computation.1 | async-start | bytes 262144 | tf_op jit(solution)/shard_map/all_to_all | solution.py:28
  67.4 6.1 %all-to-all-done.1 = f32[8,8,512]{2,1,0:T(8,128)S(1)} async-done(((f32[8,8,512]{2,1,0:T(8,128)}), f32[8,8,512]{2,1,0:T(8,128)S(1)}, u32[]{:S(2)}, u32[]{:S(2)}) %all-to-all-start.1) | async-done | bytes 131104 | tf_op jit(solution)/shard_map/all_to_all | solution.py:28
  74.5 1.6 fusion.57
  77.0 2.3 %all-gather.3.cloned.1.call-done = bf16[2048,256]{1,0:T(8,128)(2,1)} async-done(((bf16[256,256]{1,0:T(8,128)(2,1)}), bf16[2048,256]{1,0:T(8,128)(2,1)}) %all-gather.3.cloned.1.call-update) | async-done | bytes 1048592 | tf_op jit(solution)/shard_map/all_gather | solution.py:166
  79.4 1.6 convolution_convert_fusion.2
  82.2 4.0 %all-to-all-start.2 = ((bf16[4,8,2048]{2,1,0:T(8,128)(2,1)}), bf16[4,8,2048]{2,1,0:T(8,128)(2,1)S(1)}, u32[]{:S(2)}, u32[]{:S(2)}) async-start(bf16[4,8,2048]{2,1,0:T(8,128)(2,1)} %broadcast_in_dim.27), calls=%async_computation.2 | async-start | bytes 262144 | tf_op jit(solution)/shard_map/all_to_all | solution.py:28
  86.3 4.7 %all-to-all-done.2 = bf16[4,8,2048]{2,1,0:T(8,128)(2,1)S(1)} async-done(((bf16[4,8,2048]{2,1,0:T(8,128)(2,1)}), bf16[4,8,2048]{2,1,0:T(8,128)(2,1)S(1)}, u32[]{:S(2)}, u32[]{:S(2)}) %all-to-all-start.2) | async-done | bytes 131104 | tf_op jit(solution)/shard_map/all_to_all | solution.py:28
  92.2 39.2 %all_to_all.35 = bf16[128,2,512]{2,1,0:T(2,128)(2,1)S(1)} all-to-all(bf16[128,2,512]{2,1,0:T(2,128)(2,1)S(1)} %bitcast.137), channel_id=1, replica_groups=mesh['b'=8,'zp'=2,'x'=4,'c'=2,'tp'=4] {'b','zp','x','c'}, dimensions={0} | all-to-all | bytes 524288 | tf_op jit(solution)/shard_map/all_to_all | solution.py:28
  131.6 1.1 broadcast_in_dim.31
  132.6 3.5 %all-to-all-start.4 = ((bf16[4,256,512]{1,2,0:T(8,128)(2,1)}), bf16[4,256,512]{1,2,0:T(8,128)(2,1)S(1)}, u32[]{:S(2)}, u32[]{:S(2)}) async-start(bf16[4,256,512]{1,2,0:T(8,128)(2,1)} %broadcast_in_dim.31), calls=%async_computation.4 | async-start | bytes 2097152 | tf_op jit(solution)/shard_map/all_to_all | solution.py:28
  136.4 0.9 reshape.343
  137.4 13.6 %all-to-all-done.4 = bf16[4,256,512]{1,2,0:T(8,128)(2,1)S(1)} async-done(((bf16[4,256,512]{1,2,0:T(8,128)(2,1)}), bf16[4,256,512]{1,2,0:T(8,128)(2,1)S(1)}, u32[]{:S(2)}, u32[]{:S(2)}) %all-to-all-start.4) | async-done | bytes 1048608 | tf_op jit(solution)/shard_map/all_to_all | solution.py:28
  151.0 2.1 fusion.15
  153.1 2.1 convolution_convert_fusion
  156.0 2.0 fusion
  157.9 1.6 convolution_convert_fusion.1
  160.3 16.8 %all_to_all.36 = bf16[4,264,512]{2,1,0:T(8,128)(2,1)S(1)} all-to-all(bf16[4,264,512]{2,1,0:T(8,128)(2,1)S(1)} %maximum_bitcast_fusion), channel_id=1, replica_groups=mesh['b'=8,'zp'=2,'x'=4,'c'=2,'tp'=4] {'tp'}, dimensions={0} | all-to-all | bytes 2162688 | tf_op jit(solution)/shard_map/all_to_all | solution.py:28
  178.0 7.7 %all-to-all-start.6 = ((bf16[128,2,512]{2,1,0:T(2,128)(2,1)}), bf16[128,2,512]{2,1,0:T(2,128)(2,1)S(1)}, u32[]{:S(2)}, u32[]{:S(2)}) async-start(bf16[128,2,512]{2,1,0:T(2,128)(2,1)} %reshape.345), calls=%async_computation.6 | async-start | bytes 524288 | tf_op jit(solution)/shard_map/all_to_all | solution.py:28
  185.9 22.4 %all-to-all-done.6 = bf16[128,2,512]{2,1,0:T(2,128)(2,1)S(1)} async-done(((bf16[128,2,512]{2,1,0:T(2,128)(2,1)}), bf16[128,2,512]{2,1,0:T(2,128)(2,1)S(1)}, u32[]{:S(2)}, u32[]{:S(2)}) %all-to-all-start.6) | async-done | bytes 262176 | tf_op jit(solution)/shard_map/all_to_all | solution.py:28
  (130 shorter events, 18.9 us)
Async XLA Ops:
  6.5 146.6 %copy-start = (bf16[1,176,2048]{2,1,0:T(8,128)(2,1)S(1)}, bf16[1,176,2048]{2,1,0:T(8,128)(2,1)}, u32[]{:S(2)}) copy-start(bf16[1,176,2048]{2,1,0:T(8,128)(2,1)} %param.45) | copy-start | bytes 2162692
  6.5 72.8 %all-gather.3.cloned.1.call-start = ((), (), s32[]{:S(2)}) async-start(), calls=%async_computation.7 | async-start | bytes 1179648 | tf_op jit(solution)/shard_map/all_gather | solution.py:166
  42.3 16.2 %copy-start.2 = (bf16[8,1,320,128]{3,2,1,0:T(8,128)(2,1)S(1)}, bf16[8,1,320,128]{3,2,1,0:T(8,128)(2,1)}, u32[]{:S(2)}) copy-start(bf16[8,1,320,128]{3,2,1,0:T(8,128)(2,1)} %param.31) | copy-start | bytes 1966084
  45.8 16.5 %all-to-all-start = ((bf16[8,8,256]{2,1,0:T(8,128)(2,1)}), bf16[8,8,256]{2,1,0:T(8,128)(2,1)S(1)}, u32[]{:S(2)}, u32[]{:S(2)}) async-start(bf16[8,8,256]{2,1,0:T(8,128)(2,1)} %bitcast.3), calls=%async_computation | async-start | bytes 65536 | tf_op jit(solution)/shard_map/all_to_all | solution.py:28
  57.7 97.7 %all-gather.5.cloned.1.call-start = ((), (), s32[]{:S(2)}) async-start(), calls=%async_computation.8 | async-start | bytes 3538944 | tf_op jit(solution)/shard_map/all_gather | solution.py:167
  59.6 1.5 copy-start.11
  60.9 6.4 %copy-start.14 = (s32[8]{0:T(128)S(1)}, s32[8]{0:T(128)}, u32[]{:S(2)}) copy-start(s32[8]{0:T(128)} %param.33) | copy-start | bytes 100
  60.9 13.1 %copy-start.15 = (f32[64]{0:T(128)S(1)}, f32[64]{0:T(128)}, u32[]{:S(2)}) copy-start(f32[64]{0:T(128)} %param.29) | copy-start | bytes 772
  60.9 13.2 %copy-start.13 = (f32[64]{0:T(128)S(1)}, f32[64]{0:T(128)}, u32[]{:S(2)}) copy-start(f32[64]{0:T(128)} %param.28) | copy-start | bytes 772
  61.1 15.1 %copy-start.17 = (f32[2]{0:T(128)S(1)}, f32[2]{0:T(128)}, u32[]{:S(2)}) copy-start(f32[2]{0:T(128)} %param.30) | copy-start | bytes 28
  61.2 15.4 %copy-start.18 = (bf16[8,1,320,128]{3,2,1,0:T(8,128)(2,1)S(1)}, bf16[8,1,320,128]{3,2,1,0:T(8,128)(2,1)}, u32[]{:S(2)}) copy-start(bf16[8,1,320,128]{3,2,1,0:T(8,128)(2,1)} %param.32) | copy-start | bytes 1966084
  63.2 10.2 %all-to-all-start.1 = ((f32[8,8,512]{2,1,0:T(8,128)}), f32[8,8,512]{2,1,0:T(8,128)S(1)}, u32[]{:S(2)}, u32[]{:S(2)}) async-start(f32[8,8,512]{2,1,0:T(8,128)} %fusion.18), calls=%async_computation.1 | async-start | bytes 262144 | tf_op jit(solution)/shard_map/all_to_all | solution.py:28
  67.3 9.6 %copy-start.16 = (f32[128]{0:T(128)S(1)}, f32[128]{0:T(128)}, u32[]{:S(2)}) copy-start(f32[128]{0:T(128)} %param.34) | copy-start | bytes 1540
  76.6 9.7 %copy-start.12 = (f32[8,2]{0,1:T(2,128)S(1)}, f32[8,2]{0,1:T(2,128)}, u32[]{:S(2)}) copy-start(f32[8,2]{0,1:T(2,128)} %param.42) | copy-start | bytes 196
  76.9 14.2 %copy-start.7 = (bf16[8,2048]{1,0:T(8,128)(2,1)S(1)}, bf16[8,2048]{1,0:T(8,128)(2,1)}, u32[]{:S(2)}) copy-start(bf16[8,2048]{1,0:T(8,128)(2,1)} %param.23) | copy-start | bytes 98308
  76.9 14.8 %copy-start.9 = (f32[2048]{0:T(1024)S(1)}, f32[2048]{0:T(1024)}, u32[]{:S(2)}) copy-start(f32[2048]{0:T(1024)} %param.36) | copy-start | bytes 24580
  82.2 8.8 %all-to-all-start.2 = ((bf16[4,8,2048]{2,1,0:T(8,128)(2,1)}), bf16[4,8,2048]{2,1,0:T(8,128)(2,1)S(1)}, u32[]{:S(2)}, u32[]{:S(2)}) async-start(bf16[4,8,2048]{2,1,0:T(8,128)(2,1)} %broadcast_in_dim.27), calls=%async_computation.2 | async-start | bytes 262144 | tf_op jit(solution)/shard_map/all_to_all | solution.py:28
  91.8 44.3 %copy-start.5 = (bf16[8,2048]{1,0:T(8,128)(2,1)}, bf16[8,2048]{1,0:T(8,128)(2,1)S(1)}, u32[]{:S(2)}) copy-start(bf16[8,2048]{1,0:T(8,128)(2,1)S(1)} %multiply_convert_fusion.2) | copy-start | bytes 98308
  132.6 18.4 %all-to-all-start.4 = ((bf16[4,256,512]{1,2,0:T(8,128)(2,1)}), bf16[4,256,512]{1,2,0:T(8,128)(2,1)S(1)}, u32[]{:S(2)}, u32[]{:S(2)}) async-start(bf16[4,256,512]{1,2,0:T(8,128)(2,1)} %broadcast_in_dim.31), calls=%async_computation.4 | async-start | bytes 2097152 | tf_op jit(solution)/shard_map/all_to_all | solution.py:28
  136.2 17.0 %copy-start.1 = (bf16[1,2048,176]{1,2,0:T(8,128)(2,1)S(1)}, bf16[1,2048,176]{1,2,0:T(8,128)(2,1)}, u32[]{:S(2)}) copy-start(bf16[1,2048,176]{1,2,0:T(8,128)(2,1)} %param.44) | copy-start | bytes 2162692
  177.0 8.7 %copy-start.4 = (bf16[8,2048]{1,0:T(8,128)(2,1)S(1)}, bf16[8,2048]{1,0:T(8,128)(2,1)}, u32[]{:S(2)}) copy-start(bf16[8,2048]{1,0:T(8,128)(2,1)} %copy-done.3) | copy-start | bytes 98308
  177.0 8.8 %copy-start.6 = (bf16[8,2048]{1,0:T(8,128)(2,1)S(1)}, bf16[8,2048]{1,0:T(8,128)(2,1)}, u32[]{:S(2)}) copy-start(bf16[8,2048]{1,0:T(8,128)(2,1)} %copy-done.5) | copy-start | bytes 98308
  177.0 8.8 %copy-start.10 = (f32[2048]{0:T(1024)S(1)}, f32[2048]{0:T(1024)}, u32[]{:S(2)}) copy-start(f32[2048]{0:T(1024)} %param.40) | copy-start | bytes 24580
  178.0 30.3 %all-to-all-start.6 = ((bf16[128,2,512]{2,1,0:T(2,128)(2,1)}), bf16[128,2,512]{2,1,0:T(2,128)(2,1)S(1)}, u32[]{:S(2)}, u32[]{:S(2)}) async-start(bf16[128,2,512]{2,1,0:T(2,128)(2,1)} %reshape.345), calls=%async_computation.6 | async-start | bytes 524288 | tf_op jit(solution)/shard_map/all_to_all | solution.py:28
  (2 other events, 1.4 us)
Sparse Core Ops, SparseCore 0:
  43.1 36.1 all-gather.2
  81.5 36.5 all-gather.4
where the time goes:
time: 217 us; the launch traced here: 216 us
  blocking collectives  86.7 us (40%)
  waiting for transfers between devices  50 us (23%)
  starting transfers between devices  31.1 us (14%)
  local copies, waits for them, and re-layouts  16.3 us (8%)
  between operations  13.9 us (6%)
  matrix products  13.4 us (6%)
  other arithmetic  4.68 us (2%)
    all_to_all x2, blocking collectives, exchange(): return lax.all_to_all(values, axes, split_axis=0, concat_axis=0, tiled=True)  55.9 us
    all_to_all x5, waiting for transfers between devices, exchange(): return lax.all_to_all(values, axes, split_axis=0, concat_axis=0, tiled=True)  47.6 us
    all_to_all x5, starting transfers between devices, exchange(): return lax.all_to_all(values, axes, split_axis=0, concat_axis=0, tiled=True)  31.1 us
    all_gather x1, blocking collectives, shards(): held = lax.all_gather(shard, Z, axis=0, tiled=True)  30.8 us
    unnamed x46, local copies, waits for them, and re-layouts  6.65 us
  transfers between devices with their start and end apart: 7, of which 6 were waited for; matrix products, arithmetic and copies ran while one was open for 10% of the time, Pallas kernels for 0%

commit v1 on v0

--- a/solution.py
+++ b/solution.py
@@ -162,7 +162,7 @@
         ),
         axis=1,
     )
-    held = lax.all_gather(shard, Z, axis=0, tiled=True)
+    held = jnp.concatenate(lax.all_to_all(jnp.stack([shard] * lax.axis_size(Z)), Z, 0, 0), axis=0)
     out_held = lax.all_gather(held[:, 512:768], XC, axis=0, tiled=True)
     dense_held = lax.all_gather(held[:, 768:], XC, axis=0, tiled=True)
     partial_rows = jnp.dot(spread, held[:, :512], preferred_element_type=jnp.float32)

time: 217 us -> 233 us (1.074)
  waiting for transfers between devices: 50 us -> 84.7 us
  blocking collectives: 86.7 us -> 55.5 us
  starting transfers between devices: 31.1 us -> 44.9 us
    all_to_all x0 -> x1, waiting for transfers between devices: none -> 33.5 us  [shards(): lax.all_to_all(jnp.stack([shard] * lax.axis_size(Z)), Z, 0, 0)]
    all_gather x1 -> x0, blocking collectives: 30.8 us -> none  [shards(): held = lax.all_gather(shard, Z, axis=0, tiled=True)]
    all_to_all x0 -> x1, starting transfers between devices: none -> 14.8 us  [shards(): lax.all_to_all(jnp.stack([shard] * lax.axis_size(Z)), Z, 0, 0)]
    unnamed x46 -> x50, local copies, waits for them, and re-layouts: 6.65 us -> 6.7 us
  transfers between devices with their start and end apart: 7 -> 8, of which waited for: 6 -> 7; matrix products, arithmetic and copies ran while one was open for 10% -> 8% of each run, Pallas kernels for 0% -> 0%
where the time goes in v1:
time: 233 us; the launch traced here: 232 us
  waiting for transfers between devices  84.7 us (36%)
  blocking collectives  55.5 us (24%)
  starting transfers between devices  44.9 us (19%)
  local copies, waits for them, and re-layouts  17.4 us (7%)
  between operations  13.9 us (6%)
  matrix products  12.3 us (5%)
  other arithmetic  3.14 us (1%)
    all_to_all x2, blocking collectives, exchange(): return lax.all_to_all(values, axes, split_axis=0, concat_axis=0, tiled=True)  55.5 us
    all_to_all x5, waiting for transfers between devices, exchange(): return lax.all_to_all(values, axes, split_axis=0, concat_axis=0, tiled=True)  47.5 us
    all_to_all x1, waiting for transfers between devices, shards(): lax.all_to_all(jnp.stack([shard] * lax.axis_size(Z)), Z, 0, 0)  33.5 us
    all_to_all x5, starting transfers between devices, exchange(): return lax.all_to_all(values, axes, split_axis=0, concat_axis=0, tiled=True)  30.1 us
    all_to_all x1, starting transfers between devices, shards(): lax.all_to_all(jnp.stack([shard] * lax.axis_size(Z)), Z, 0, 0)  14.8 us
    unnamed x50, local copies, waits for them, and re-layouts  6.7 us
  transfers between devices with their start and end apart: 8, of which 7 were waited for; matrix products, arithmetic and copies ran while one was open for 8% of the time, Pallas kernels for 0%

profile of v1, /device:TPU:33, one launch (start us, length us, event | category | flops | bytes accessed | tf_op | source)
XLA Modules:
  0.0 231.8 jit_solution(7966165794464255305)
XLA Ops:
  11.5 1.0 stack.2
  12.5 14.8 %all-to-all-start.1 = ((bf16[16,16,1536]{2,1,0:T(8,128)(2,1)}), bf16[16,16,1536]{2,1,0:T(8,128)(2,1)S(1)}, u32[]{:S(2)}, u32[]{:S(2)}) async-start(bf16[16,16,1536]{2,1,0:T(8,128)(2,1)} %stack.2), calls=%async_computation.1 | async-start | bytes 1572864 | tf_op jit(solution)/shard_map/all_to_all | solution.py:165
  27.4 33.5 %all-to-all-done.1 = bf16[16,16,1536]{2,1,0:T(8,128)(2,1)S(1)} async-done(((bf16[16,16,1536]{2,1,0:T(8,128)(2,1)}), bf16[16,16,1536]{2,1,0:T(8,128)(2,1)S(1)}, u32[]{:S(2)}, u32[]{:S(2)}) %all-to-all-start.1) | async-done | bytes 786464 | tf_op jit(solution)/shard_map/all_to_all | solution.py:165
  62.9 10.9 %all-to-all-start = ((bf16[8,8,256]{2,1,0:T(8,128)(2,1)}), bf16[8,8,256]{2,1,0:T(8,128)(2,1)S(1)}, u32[]{:S(2)}, u32[]{:S(2)}) async-start(bf16[8,8,256]{2,1,0:T(8,128)(2,1)} %bitcast.3), calls=%async_computation | async-start | bytes 65536 | tf_op jit(solution)/shard_map/all_to_all | solution.py:28
  73.8 1.2 copy.94
  75.3 1.3 convert_multiply_fusion
  76.9 1.6 all-to-all-done
  79.4 4.0 %all-to-all-start.2 = ((f32[8,8,512]{2,1,0:T(8,128)}), f32[8,8,512]{2,1,0:T(8,128)S(1)}, u32[]{:S(2)}, u32[]{:S(2)}) async-start(f32[8,8,512]{2,1,0:T(8,128)} %fusion.18), calls=%async_computation.2 | async-start | bytes 262144 | tf_op jit(solution)/shard_map/all_to_all | solution.py:28
  84.3 5.2 %all-to-all-done.2 = f32[8,8,512]{2,1,0:T(8,128)S(1)} async-done(((f32[8,8,512]{2,1,0:T(8,128)}), f32[8,8,512]{2,1,0:T(8,128)S(1)}, u32[]{:S(2)}, u32[]{:S(2)}) %all-to-all-start.2) | async-done | bytes 131104 | tf_op jit(solution)/shard_map/all_to_all | solution.py:28
  91.9 3.6 %all-gather.3.cloned.1.call-done = bf16[2048,256]{1,0:T(8,128)(2,1)} async-done(((bf16[256,256]{1,0:T(8,128)(2,1)}), bf16[2048,256]{1,0:T(8,128)(2,1)}) %all-gather.3.cloned.1.call-update) | async-done | bytes 1048592 | tf_op jit(solution)/shard_map/all_gather | solution.py:166
  95.5 1.6 convolution_convert_fusion.2
  98.4 4.0 %all-to-all-start.3 = ((bf16[4,8,2048]{2,1,0:T(8,128)(2,1)}), bf16[4,8,2048]{2,1,0:T(8,128)(2,1)S(1)}, u32[]{:S(2)}, u32[]{:S(2)}) async-start(bf16[4,8,2048]{2,1,0:T(8,128)(2,1)} %broadcast_in_dim.27), calls=%async_computation.3 | async-start | bytes 262144 | tf_op jit(solution)/shard_map/all_to_all | solution.py:28
  102.4 4.7 %all-to-all-done.3 = bf16[4,8,2048]{2,1,0:T(8,128)(2,1)S(1)} async-done(((bf16[4,8,2048]{2,1,0:T(8,128)(2,1)}), bf16[4,8,2048]{2,1,0:T(8,128)(2,1)S(1)}, u32[]{:S(2)}, u32[]{:S(2)}) %all-to-all-start.3) | async-done | bytes 131104 | tf_op jit(solution)/shard_map/all_to_all | solution.py:28
  108.3 38.7 %all_to_all.40 = bf16[128,2,512]{2,1,0:T(2,128)(2,1)S(1)} all-to-all(bf16[128,2,512]{2,1,0:T(2,128)(2,1)S(1)} %bitcast.141), channel_id=1, replica_groups=mesh['b'=8,'zp'=2,'x'=4,'c'=2,'tp'=4] {'b','zp','x','c'}, dimensions={0} | all-to-all | bytes 524288 | tf_op jit(solution)/shard_map/all_to_all | solution.py:28
  147.3 1.1 broadcast_in_dim.31
  148.3 3.5 %all-to-all-start.5 = ((bf16[4,256,512]{1,2,0:T(8,128)(2,1)}), bf16[4,256,512]{1,2,0:T(8,128)(2,1)S(1)}, u32[]{:S(2)}, u32[]{:S(2)}) async-start(bf16[4,256,512]{1,2,0:T(8,128)(2,1)} %broadcast_in_dim.31), calls=%async_computation.5 | async-start | bytes 2097152 | tf_op jit(solution)/shard_map/all_to_all | solution.py:28
  153.1 13.6 %all-to-all-done.5 = bf16[4,256,512]{1,2,0:T(8,128)(2,1)S(1)} async-done(((bf16[4,256,512]{1,2,0:T(8,128)(2,1)}), bf16[4,256,512]{1,2,0:T(8,128)(2,1)S(1)}, u32[]{:S(2)}, u32[]{:S(2)}) %all-to-all-start.5) | async-done | bytes 1048608 | tf_op jit(solution)/shard_map/all_to_all | solution.py:28
  166.7 2.1 fusion.15
  168.8 2.1 convolution_convert_fusion
  171.7 2.0 fusion
  173.7 1.6 convolution_convert_fusion.1
  176.0 16.8 %all_to_all.41 = bf16[4,264,512]{2,1,0:T(8,128)(2,1)S(1)} all-to-all(bf16[4,264,512]{2,1,0:T(8,128)(2,1)S(1)} %maximum_bitcast_fusion), channel_id=1, replica_groups=mesh['b'=8,'zp'=2,'x'=4,'c'=2,'tp'=4] {'tp'}, dimensions={0} | all-to-all | bytes 2162688 | tf_op jit(solution)/shard_map/all_to_all | solution.py:28
  193.7 7.7 %all-to-all-start.7 = ((bf16[128,2,512]{2,1,0:T(2,128)(2,1)}), bf16[128,2,512]{2,1,0:T(2,128)(2,1)S(1)}, u32[]{:S(2)}, u32[]{:S(2)}) async-start(bf16[128,2,512]{2,1,0:T(2,128)(2,1)} %reshape.351), calls=%async_computation.7 | async-start | bytes 524288 | tf_op jit(solution)/shard_map/all_to_all | solution.py:28
  201.7 22.4 %all-to-all-done.7 = bf16[128,2,512]{2,1,0:T(2,128)(2,1)S(1)} async-done(((bf16[128,2,512]{2,1,0:T(2,128)(2,1)}), bf16[128,2,512]{2,1,0:T(2,128)(2,1)S(1)}, u32[]{:S(2)}, u32[]{:S(2)}) %all-to-all-start.7) | async-done | bytes 262176 | tf_op jit(solution)/shard_map/all_to_all | solution.py:28
  (136 shorter events, 19.0 us)
Async XLA Ops:
  6.5 162.3 %copy-start = (bf16[1,176,2048]{2,1,0:T(8,128)(2,1)S(1)}, bf16[1,176,2048]{2,1,0:T(8,128)(2,1)}, u32[]{:S(2)}) copy-start(bf16[1,176,2048]{2,1,0:T(8,128)(2,1)} %param.45) | copy-start | bytes 2162692
  6.5 20.8 %copy-start.8 = (bf16[8,2048]{1,0:T(8,128)(2,1)S(1)}, bf16[8,2048]{1,0:T(8,128)(2,1)}, u32[]{:S(2)}) copy-start(bf16[8,2048]{1,0:T(8,128)(2,1)} %param.23) | copy-start | bytes 98308
  6.5 55.2 %copy-start.10 = (f32[2048]{0:T(1024)S(1)}, f32[2048]{0:T(1024)}, u32[]{:S(2)}) copy-start(f32[2048]{0:T(1024)} %param.24) | copy-start | bytes 24580
  12.4 61.3 %copy-start.3 = (bf16[8,1,320,128]{3,2,1,0:T(8,128)(2,1)S(1)}, bf16[8,1,320,128]{3,2,1,0:T(8,128)(2,1)}, u32[]{:S(2)}) copy-start(bf16[8,1,320,128]{3,2,1,0:T(8,128)(2,1)} %param.31) | copy-start | bytes 1966084
  12.5 48.5 %all-to-all-start.1 = ((bf16[16,16,1536]{2,1,0:T(8,128)(2,1)}), bf16[16,16,1536]{2,1,0:T(8,128)(2,1)S(1)}, u32[]{:S(2)}, u32[]{:S(2)}) async-start(bf16[16,16,1536]{2,1,0:T(8,128)(2,1)} %stack.2), calls=%async_computation.1 | async-start | bytes 1572864 | tf_op jit(solution)/shard_map/all_to_all | solution.py:165
  27.2 47.7 %copy-start.13 = (s32[8,2]{0,1:T(2,128)S(1)}, s32[8,2]{0,1:T(2,128)}, u32[]{:S(2)}) copy-start(s32[8,2]{0,1:T(2,128)} %param.41) | copy-start | bytes 196
  27.2 68.3 %all-gather.3.cloned.1.call-start = ((), (), s32[]{:S(2)}) async-start(), calls=%async_computation.8 | async-start | bytes 1179648 | tf_op jit(solution)/shard_map/all_gather | solution.py:166
  62.9 15.6 %all-to-all-start = ((bf16[8,8,256]{2,1,0:T(8,128)(2,1)}), bf16[8,8,256]{2,1,0:T(8,128)(2,1)S(1)}, u32[]{:S(2)}, u32[]{:S(2)}) async-start(bf16[8,8,256]{2,1,0:T(8,128)(2,1)} %bitcast.3), calls=%async_computation | async-start | bytes 65536 | tf_op jit(solution)/shard_map/all_to_all | solution.py:28
  76.6 13.4 %copy-start.17 = (f32[64]{0:T(128)S(1)}, f32[64]{0:T(128)}, u32[]{:S(2)}) copy-start(f32[64]{0:T(128)} %param.29) | copy-start | bytes 772
  76.6 13.5 %copy-start.15 = (f32[64]{0:T(128)S(1)}, f32[64]{0:T(128)}, u32[]{:S(2)}) copy-start(f32[64]{0:T(128)} %param.28) | copy-start | bytes 772
  76.8 13.6 %copy-start.1 = (bf16[8,1,320,128]{2,3,0,1:T(8,128)(2,1)S(1)}, bf16[8,1,320,128]{2,3,0,1:T(8,128)(2,1)}, u32[]{:S(2)}) copy-start(bf16[8,1,320,128]{2,3,0,1:T(8,128)(2,1)} %copy.94) | copy-start | bytes 1966084
  79.4 10.1 %all-to-all-start.2 = ((f32[8,8,512]{2,1,0:T(8,128)}), f32[8,8,512]{2,1,0:T(8,128)S(1)}, u32[]{:S(2)}, u32[]{:S(2)}) async-start(f32[8,8,512]{2,1,0:T(8,128)} %fusion.18), calls=%async_computation.2 | async-start | bytes 262144 | tf_op jit(solution)/shard_map/all_to_all | solution.py:28
  83.4 87.7 %all-gather.5.cloned.1.call-start = ((), (), s32[]{:S(2)}) async-start(), calls=%async_computation.9 | async-start | bytes 3538944 | tf_op jit(solution)/shard_map/all_gather | solution.py:167
  83.4 7.6 %copy-start.19 = (f32[2]{0:T(128)S(1)}, f32[2]{0:T(128)}, u32[]{:S(2)}) copy-start(f32[2]{0:T(128)} %param.30) | copy-start | bytes 28
  91.4 11.0 %copy-start.14 = (f32[8,2]{0,1:T(2,128)S(1)}, f32[8,2]{0,1:T(2,128)}, u32[]{:S(2)}) copy-start(f32[8,2]{0,1:T(2,128)} %param.42) | copy-start | bytes 196
  91.8 16.1 %copy-start.11 = (f32[2048]{0:T(1024)S(1)}, f32[2048]{0:T(1024)}, u32[]{:S(2)}) copy-start(f32[2048]{0:T(1024)} %param.36) | copy-start | bytes 24580
  98.4 8.8 %all-to-all-start.3 = ((bf16[4,8,2048]{2,1,0:T(8,128)(2,1)}), bf16[4,8,2048]{2,1,0:T(8,128)(2,1)S(1)}, u32[]{:S(2)}, u32[]{:S(2)}) async-start(bf16[4,8,2048]{2,1,0:T(8,128)(2,1)} %broadcast_in_dim.27), calls=%async_computation.3 | async-start | bytes 262144 | tf_op jit(solution)/shard_map/all_to_all | solution.py:28
  107.9 43.9 %copy-start.6 = (bf16[8,2048]{1,0:T(8,128)(2,1)}, bf16[8,2048]{1,0:T(8,128)(2,1)S(1)}, u32[]{:S(2)}) copy-start(bf16[8,2048]{1,0:T(8,128)(2,1)S(1)} %multiply_convert_fusion.2) | copy-start | bytes 98308
  148.3 18.4 %all-to-all-start.5 = ((bf16[4,256,512]{1,2,0:T(8,128)(2,1)}), bf16[4,256,512]{1,2,0:T(8,128)(2,1)S(1)}, u32[]{:S(2)}, u32[]{:S(2)}) async-start(bf16[4,256,512]{1,2,0:T(8,128)(2,1)} %broadcast_in_dim.31), calls=%async_computation.5 | async-start | bytes 2097152 | tf_op jit(solution)/shard_map/all_to_all | solution.py:28
  151.9 17.0 %copy-start.2 = (bf16[1,2048,176]{1,2,0:T(8,128)(2,1)S(1)}, bf16[1,2048,176]{1,2,0:T(8,128)(2,1)}, u32[]{:S(2)}) copy-start(bf16[1,2048,176]{1,2,0:T(8,128)(2,1)} %param.44) | copy-start | bytes 2162692
  192.7 8.7 %copy-start.5 = (bf16[8,2048]{1,0:T(8,128)(2,1)S(1)}, bf16[8,2048]{1,0:T(8,128)(2,1)}, u32[]{:S(2)}) copy-start(bf16[8,2048]{1,0:T(8,128)(2,1)} %copy-done.4) | copy-start | bytes 98308
  192.7 8.8 %copy-start.7 = (bf16[8,2048]{1,0:T(8,128)(2,1)S(1)}, bf16[8,2048]{1,0:T(8,128)(2,1)}, u32[]{:S(2)}) copy-start(bf16[8,2048]{1,0:T(8,128)(2,1)} %copy-done.6) | copy-start | bytes 98308
  192.7 8.8 %copy-start.12 = (f32[2048]{0:T(1024)S(1)}, f32[2048]{0:T(1024)}, u32[]{:S(2)}) copy-start(f32[2048]{0:T(1024)} %param.40) | copy-start | bytes 24580
  193.7 30.3 %all-to-all-start.7 = ((bf16[128,2,512]{2,1,0:T(2,128)(2,1)}), bf16[128,2,512]{2,1,0:T(2,128)(2,1)S(1)}, u32[]{:S(2)}, u32[]{:S(2)}) async-start(bf16[128,2,512]{2,1,0:T(2,128)(2,1)} %reshape.351), calls=%async_computation.7 | async-start | bytes 524288 | tf_op jit(solution)/shard_map/all_to_all | solution.py:28
  (5 other events, 22.8 us)
Sparse Core Ops, SparseCore 0:
  61.8 33.6 all-gather.2
  97.6 36.0 all-gather.4
